TPU v7x, 512 devices: a whole 4x8x8 slice. The times are simulated.
512 devices in a mesh: dp: 4 (over x), kv: 64 (over z, y), tp: 2 (over core).
Axes of the slice: x: 4, y: 8, z: 8, core: 2. Of those that a mesh axis runs over, the one named last changes fastest.
Arguments:
- tokens: bfloat16 [512, 2048], P('dp', ('kv', 'tp')), parts along dimension 0, may hold values from -8 to 8
- mlp1_gain: float32 [2048], replicated, may hold values from 0.1 to 1.9
- mlp1_gate: bfloat16 [2048, 5632], P(None, ('kv', 'tp')), may hold values from -0.125 to 0.125
- mlp1_up: bfloat16 [2048, 5632], P(None, ('kv', 'tp')), may hold values from -0.125 to 0.125
- mlp1_down: bfloat16 [5632, 2048], P(('kv', 'tp')), may hold values from -0.3125 to 0.3125
- mixer_gain: float32 [2048], replicated, may hold values from 0.1 to 1.9
- proj_z: bfloat16 [2048, 2048], P('kv', 'tp'), may hold values from -0.125 to 0.125
- proj_x: bfloat16 [2048, 2048], P('kv', 'tp'), may hold values from -0.125 to 0.125
- proj_bc: bfloat16 [2048, 2, 512], P('kv', None, 'tp'), may hold values from -0.125 to 0.125
- proj_dt: bfloat16 [2048, 32], P('kv', 'tp'), may hold values from -0.125 to 0.125
- conv_x: bfloat16 [4, 2048], P(None, 'tp'), may hold values from -3 to 3
- conv_bc: bfloat16 [4, 2, 512], P(None, None, 'tp'), may hold values from -3 to 3
- window_x: bfloat16 [512, 3, 2048], P(('dp', 'kv'), None, 'tp'), parts along dimension 0, may hold values from -6 to 6
- window_bc: bfloat16 [512, 3, 2, 512], P(('dp', 'kv'), None, None, 'tp'), parts along dimension 0, may hold values from -6 to 6
- ssm_state: float32 [512, 32, 64, 128], P(('dp', 'kv'), 'tp'), parts along dimension 0, may hold values from -0.8 to 0.8
- dt_bias: float32 [32], P('tp'), may hold values from -4 to 0
- log_rate: float32 [32], P('tp'), may hold values from 0 to 2.77
- skip_gain: float32 [32], P('tp'), may hold values from 0.25 to 2
- group_gain: float32 [2048], P('tp'), may hold values from 0.1 to 1.9
- out_weight: bfloat16 [2048, 2048], P('tp', 'kv'), may hold values from -0.125 to 0.125
- mlp2_gain: float32 [2048], replicated, may hold values from 0.1 to 1.9
- mlp2_gate: bfloat16 [2048, 5632], P(None, ('kv', 'tp')), may hold values from -0.125 to 0.125
- mlp2_up: bfloat16 [2048, 5632], P(None, ('kv', 'tp')), may hold values from -0.125 to 0.125
- mlp2_down: bfloat16 [5632, 2048], P(('kv', 'tp')), may hold values from -0.3125 to 0.3125
Outputs:
- result: bfloat16 [512, 2048], P('dp', ('kv', 'tp')), parts along dimension 0
- new_state: float32 [512, 32, 64, 128], P(('dp', 'kv'), 'tp'), parts along dimension 0
- new_window_x: bfloat16 [512, 3, 2048], P(('dp', 'kv'), None, 'tp'), parts along dimension 0
- new_window_bc: bfloat16 [512, 3, 2, 512], P(('dp', 'kv'), None, None, 'tp'), parts along dimension 0
There are 4 independent parts, one for each index of `dp`. A program takes and returns all parts, laid end to end along the dimension named above; an argument that names none is the same for every part. Nothing has to cross between parts.
All inputs are finite; a program needn't handle non-finite values.
Results may differ from a plain program's by a relative error of at most 0.013.
Values may be sent and summed in bfloat16 or wider, within the bound.
A program may use at most 64 MiB of HBM per device.

v0:
```python
import jax
import jax.numpy as jnp
from jax import lax
from jax.sharding import Mesh
from jax.sharding import PartitionSpec as P

KV = ("kv_0", "kv_1")
KV_TP = ("kv_0", "kv_1", "tp")
DP_KV = ("dp", "kv_0", "kv_1")


EPS = 1e-06


def in_order(tiles, dim):
    tiles = jnp.moveaxis(tiles, 0, dim)
    shape = tiles.shape
    return tiles.reshape(*shape[:dim], shape[dim] * shape[dim + 1], *shape[dim + 2 :])


def copy_for_each(array, axis):
    size = lax.axis_size(axis)
    return lax.all_to_all(
        jnp.broadcast_to(array[None], (size, *array.shape)), axis, 0, 0, tiled=True
    )


def gather_directly(array, axis, dim):
    return in_order(copy_for_each(array, axis), dim)


def cut_along(array, dim, size):
    shape = array.shape
    tiles = array.reshape(*shape[:dim], size, shape[dim] // size, *shape[dim + 1 :])
    return jnp.moveaxis(tiles, dim, 0)


def sum_at_owner(array, axis, dim):
    size = lax.axis_size(axis)
    tiles = lax.all_to_all(cut_along(array, dim, size), axis, 0, 0, tiled=True)
    return jnp.sum(tiles.astype(jnp.float32), axis=0)


def sum_at_owner_2(array, axis, dim):
    tiles = cut_along(array, dim, lax.axis_size(axis))
    arrived = lax.all_to_all(tiles, axis, split_axis=0, concat_axis=0, tiled=True)
    return arrived.sum(axis=0)


def by_axis(array, axes):
    for axis in axes:
        array = lax.psum(array, axis)
    return array


def norm_rows(values, scale_gain):
    floats = values.astype(jnp.float32)
    factor = lax.rsqrt(jnp.mean(floats * floats, axis=-1, keepdims=True) + EPS)
    return (floats * factor * scale_gain).astype(jnp.bfloat16)


def half_mlp(columns, scale_gain, gate_weight, up_weight, down_weight):
    paired = gather_directly(columns, "tp", 1)
    gathered = gather_directly(paired, KV, 1)
    normed = norm_rows(gathered, scale_gain)
    gate_part = jnp.dot(normed, gate_weight, preferred_element_type=jnp.float32)
    up_part = jnp.dot(normed, up_weight, preferred_element_type=jnp.float32)
    hidden = (jax.nn.silu(gate_part) * up_part).astype(jnp.bfloat16)
    partial_sums = jnp.dot(hidden, down_weight, preferred_element_type=jnp.float32)
    paired_sums = sum_at_owner(partial_sums.astype(jnp.bfloat16), KV, 1)
    summed = sum_at_owner_2(paired_sums, "tp", 1)
    return (columns.astype(jnp.float32) + 0.5 * summed).astype(jnp.bfloat16)


def per_device(
    tokens,
    mlp1_gain,
    mlp1_gate,
    mlp1_up,
    mlp1_down,
    mixer_gain,
    proj_z,
    proj_x,
    proj_bc,
    proj_dt,
    conv_x,
    conv_bc,
    window_x,
    window_bc,
    ssm_state,
    dt_bias,
    log_rate,
    skip_gain,
    group_gain,
    out_weight,
    mlp2_gain,
    mlp2_gate,
    mlp2_up,
    mlp2_down,
):
    after_first = half_mlp(tokens, mlp1_gain, mlp1_gate, mlp1_up, mlp1_down)
    kv_width = proj_z.shape[0]
    kv_offset = lax.axis_index(KV) * kv_width
    own_cols = gather_directly(after_first, "tp", 1)
    floats = after_first.astype(jnp.float32)
    squares = by_axis(jnp.sum(floats * floats, axis=1), KV_TP)
    model_width = kv_width * lax.axis_size(KV)
    factor = lax.rsqrt(squares / model_width + EPS)
    gain_cols = lax.dynamic_slice_in_dim(mixer_gain, kv_offset, kv_width, 0)
    normed = (own_cols.astype(jnp.float32) * factor[:, None] * gain_cols).astype(jnp.bfloat16)
    inner_width = proj_z.shape[1]
    group_width = proj_bc.shape[2]
    joined = jnp.concatenate(
        [proj_z, proj_x, proj_bc.reshape(kv_width, 2 * group_width), proj_dt], axis=1
    )
    own_seqs = window_x.shape[0]
    projected = sum_at_owner(
        jnp.dot(normed, joined, preferred_element_type=jnp.float32).astype(jnp.bfloat16), KV, 0
    )
    gate_z = projected[:, :inner_width].astype(jnp.bfloat16)
    x_new = projected[:, inner_width : 2 * inner_width].astype(jnp.bfloat16)
    bc_end = 2 * inner_width + 2 * group_width
    bc_new = (
        projected[:, 2 * inner_width : bc_end]
        .astype(jnp.bfloat16)
        .reshape(own_seqs, 2, group_width)
    )
    rate_raw = projected[:, bc_end:]
    full_x = jnp.concatenate([window_x, x_new[:, None]], axis=1)
    full_bc = jnp.concatenate([window_bc, bc_new[:, None]], axis=1)
    mixed_x = jax.nn.silu(
        jnp.einsum("sji,ji->si", full_x.astype(jnp.float32), conv_x.astype(jnp.float32))
    )
    mixed_bc = jax.nn.silu(
        jnp.einsum("sjci,jci->sci", full_bc.astype(jnp.float32), conv_bc.astype(jnp.float32))
    )
    heads = proj_dt.shape[1]
    state_size = ssm_state.shape[3]
    groups = group_width // state_size
    head_dim = inner_width // heads
    repeat = heads // groups
    inputs_x = mixed_x.reshape(own_seqs, heads, head_dim)
    keys_b = jnp.repeat(mixed_bc[:, 0].reshape(own_seqs, groups, state_size), repeat, axis=1)
    reads_c = jnp.repeat(mixed_bc[:, 1].reshape(own_seqs, groups, state_size), repeat, axis=1)
    step_size = jax.nn.softplus(rate_raw + dt_bias)
    retain = jnp.exp(-step_size * jnp.exp(log_rate))
    new_state = (
        retain[:, :, None, None] * ssm_state
        + (step_size[:, :, None] * inputs_x)[:, :, :, None] * keys_b[:, :, None, :]
    )
    readout = jnp.einsum("shpn,shn->shp", new_state, reads_c) + skip_gain[None, :, None] * inputs_x
    gated = readout.reshape(own_seqs, inner_width) * jax.nn.silu(gate_z.astype(jnp.float32))
    grouped = gated.reshape(own_seqs, groups, inner_width // groups)
    grouped = grouped * lax.rsqrt(jnp.mean(grouped * grouped, axis=-1, keepdims=True) + EPS)
    mixed = (grouped.reshape(own_seqs, inner_width) * group_gain).astype(jnp.bfloat16)
    partial_out = jnp.dot(
        gather_directly(mixed, KV, 0), out_weight, preferred_element_type=jnp.float32
    )
    summed_out = sum_at_owner(partial_out.astype(jnp.bfloat16), "tp", 1)
    after_mixer = (after_first.astype(jnp.float32) + summed_out).astype(jnp.bfloat16)
    result = half_mlp(after_mixer, mlp2_gain, mlp2_gate, mlp2_up, mlp2_down)
    return (result, new_state, full_x[:, 1:], full_bc[:, 1:])


def solution(mesh):
    torus = Mesh(
        mesh.devices.reshape(mesh.shape["dp"], 8, 8, mesh.shape["tp"]), ("dp", "kv_0", "kv_1", "tp")
    )
    placed = (
        P("dp", KV_TP),
        P(),
        P(None, KV_TP),
        P(None, KV_TP),
        P(KV_TP, None),
        P(),
        P(KV, "tp"),
        P(KV, "tp"),
        P(KV, None, "tp"),
        P(KV, "tp"),
        P(None, "tp"),
        P(None, None, "tp"),
        P(DP_KV, None, "tp"),
        P(DP_KV, None, None, "tp"),
        P(DP_KV, "tp", None, None),
        P("tp"),
        P("tp"),
        P("tp"),
        P("tp"),
        P("tp", KV),
        P(),
        P(None, KV_TP),
        P(None, KV_TP),
        P(KV_TP, None),
    )
    return jax.shard_map(
        per_device,
        mesh=torus,
        in_specs=placed,
        out_specs=(
            P("dp", KV_TP),
            P(DP_KV, "tp", None, None),
            P(DP_KV, None, "tp"),
            P(DP_KV, None, None, "tp"),
        ),
        check_vma=False,
    )
```

profile of v0, /device:TPU:1, one launch (start us, length us, event | category | flops | bytes accessed | tf_op | source)
XLA Modules:
  0.0 228.9 jit_solution(9749636929286779759)
XLA Ops:
  0.6 0.0 copy-start
  0.6 0.7 broadcast_in_dim.22
  1.4 10.2 %all_to_all.60 = bf16[2,128,16]{1,2,0:T(8,128)(2,1)S(1)} all-to-all(bf16[2,128,16]{1,2,0:T(8,128)(2,1)S(1)} %broadcast_in_dim.22), channel_id=1, replica_groups=mesh['dp'=4,'kv_0'=8,'kv_1'=8,'tp'=2] {'tp'}, dimensions={0} | all-to-all | bytes 16384 | tf_op jit(solution)/shard_map/all_to_all | solution.py:23
  11.6 0.1 broadcast_in_dim.24
  11.6 28.4 %all_to_all.61 = bf16[64,128,32]{1,2,0:T(8,128)(2,1)S(1)} all-to-all(bf16[64,128,32]{1,2,0:T(8,128)(2,1)S(1)} %broadcast_in_dim.24), channel_id=1, replica_groups=mesh['dp'=4,'kv_0'=8,'kv_1'=8,'tp'=2] {'kv_0','kv_1'}, dimensions={0} | all-to-all | bytes 1048576 | tf_op jit(solution)/shard_map/all_to_all | solution.py:23
  40.0 0.3 multiply_reduce_fusion.1
  40.3 0.3 fusion.5
  40.7 0.3 copy-done.3
  41.0 0.2 fusion.43
  41.2 0.5 convolution_convert_fusion.2
  41.7 0.0 copy-start.12
  41.8 1.0 copy.32
  42.8 6.7 %all-to-all-start.2 = ((bf16[64,128,32]{1,2,0:T(8,128)(2,1)}), bf16[64,128,32]{1,2,0:T(8,128)(2,1)S(1)}, u32[]{:S(2)}, u32[]{:S(2)}) async-start(bf16[64,128,32]{1,2,0:T(8,128)(2,1)} %bitcast.9), calls=%async_computation.2 | async-start | bytes 1048576 | tf_op jit(solution)/shard_map/all_to_all | solution.py:40
  49.5 0.1 copy.33
  49.6 0.8 dynamic_slice.3
  50.4 15.7 %all-to-all-done.2 = bf16[64,128,32]{1,2,0:T(8,128)(2,1)S(1)} async-done(((bf16[64,128,32]{1,2,0:T(8,128)(2,1)}), bf16[64,128,32]{1,2,0:T(8,128)(2,1)S(1)}, u32[]{:S(2)}, u32[]{:S(2)}) %all-to-all-start.2) | async-done | bytes 524320 | tf_op jit(solution)/shard_map/all_to_all | solution.py:40
  66.1 0.1 convert_reduce_fusion.2
  66.2 7.3 %all_to_all.62 = f32[2,128,16]{1,2,0:T(8,128)S(1)} all-to-all(f32[2,128,16]{1,2,0:T(8,128)S(1)} %bitcast.111), channel_id=1, replica_groups=mesh['dp'=4,'kv_0'=8,'kv_1'=8,'tp'=2] {'tp'}, dimensions={0} | all-to-all | bytes 32768 | tf_op jit(solution)/shard_map/all_to_all | solution.py:46
  73.5 0.6 broadcast_in_dim.25
  74.1 3.6 %all-to-all-start.4 = ((bf16[2,128,16]{1,2,0:T(8,128)(2,1)}), bf16[2,128,16]{1,2,0:T(8,128)(2,1)S(1)}, u32[]{:S(2)}, u32[]{:S(2)}) async-start(bf16[2,128,16]{1,2,0:T(8,128)(2,1)} %broadcast_in_dim.25), calls=%async_computation.4 | async-start | bytes 16384 | tf_op jit(solution)/shard_map/all_to_all | solution.py:23
  77.7 11.3 %psum.21 = f32[128]{0:T(128)S(1)} all-reduce(f32[128]{0:T(128)S(1)} %get-tuple-element.8), channel_id=1, replica_groups=mesh['dp'=4,'kv_0'=8,'kv_1'=8,'tp'=2] {'kv_0'}, use_global_device_ids=true, to_apply=%region_4.5 | all-reduce | flops 128 | bytes 1024 | tf_op jit(solution)/shard_map/psum | solution.py:52
  89.0 12.0 %psum.22 = f32[128]{0:T(128)S(1)} all-reduce(f32[128]{0:T(128)S(1)} %psum.21), channel_id=1, replica_groups=mesh['dp'=4,'kv_0'=8,'kv_1'=8,'tp'=2] {'kv_1'}, use_global_device_ids=true, to_apply=%region_5.6 | all-reduce | flops 128 | bytes 1024 | tf_op jit(solution)/shard_map/psum | solution.py:52
  101.1 9.4 %psum.23 = f32[128]{0:T(128)S(1)} all-reduce(f32[128]{0:T(128)S(1)} %psum.22), channel_id=1, replica_groups=mesh['dp'=4,'kv_0'=8,'kv_1'=8,'tp'=2] {'tp'}, use_global_device_ids=true, to_apply=%region_6.7 | all-reduce | flops 128 | bytes 1024 | tf_op jit(solution)/shard_map/psum | solution.py:52
  110.5 0.1 fusion.24
  110.6 0.4 convolution_convert_fusion
  111.0 0.3 copy.34
  111.3 0.0 copy-start.17
  111.4 1.1 reshape.103
  112.5 7.7 %all-to-all-start.5 = ((bf16[64,2,2576]{2,1,0:T(2,128)(2,1)}), bf16[64,2,2576]{2,1,0:T(2,128)(2,1)S(1)}, u32[]{:S(2)}, u32[]{:S(2)}) async-start(bf16[64,2,2576]{2,1,0:T(2,128)(2,1)} %reshape.103), calls=%async_computation.5 | async-start | bytes 1376256 | tf_op jit(solution)/shard_map/all_to_all | solution.py:40
  120.2 20.5 %all-to-all-done.5 = bf16[64,2,2576]{2,1,0:T(2,128)(2,1)S(1)} async-done(((bf16[64,2,2576]{2,1,0:T(2,128)(2,1)}), bf16[64,2,2576]{2,1,0:T(2,128)(2,1)S(1)}, u32[]{:S(2)}, u32[]{:S(2)}) %all-to-all-start.5) | async-done | bytes 659488 | tf_op jit(solution)/shard_map/all_to_all | solution.py:40
  140.8 0.6 convert_reduce_fusion
  141.5 0.1 reshape.104
  141.7 0.1 broadcast_multiply_fusion
  141.8 0.4 multiply_add_fusion
  142.2 0.0 copy-start.21
  142.2 0.0 copy-start.20
  142.2 0.0 copy-start.10
  142.2 0.4 fusion.44
  142.6 0.3 copy-done.21
  142.9 0.1 multiply_add_fusion.1
  142.9 0.1 reshape.106
  143.1 0.1 reduce_sum.95
  143.2 0.1 broadcast_bitcast_fusion.1
  143.3 0.1 broadcast_in_dim.29
  143.4 19.3 %all_to_all.63 = bf16[64,2,1024]{2,1,0:T(2,128)(2,1)S(1)} all-to-all(bf16[64,2,1024]{2,1,0:T(2,128)(2,1)S(1)} %broadcast_in_dim.29), channel_id=1, replica_groups=mesh['dp'=4,'kv_0'=8,'kv_1'=8,'tp'=2] {'kv_0','kv_1'}, dimensions={0} | all-to-all | bytes 524288 | tf_op jit(solution)/shard_map/all_to_all | solution.py:23
  162.8 0.1 reshape.107
  162.9 0.2 convolution_convert_fusion.3
  163.1 6.7 %all_to_all.64 = bf16[2,128,16]{1,2,0:T(8,128)(2,1)S(1)} all-to-all(bf16[2,128,16]{1,2,0:T(8,128)(2,1)S(1)} %bitcast.117), channel_id=1, replica_groups=mesh['dp'=4,'kv_0'=8,'kv_1'=8,'tp'=2] {'tp'}, dimensions={0} | all-to-all | bytes 16384 | tf_op jit(solution)/shard_map/all_to_all | solution.py:40
  169.7 3.7 %all_to_all.65 = bf16[2,128,16]{1,2,0:T(8,128)(2,1)S(1)} all-to-all(bf16[2,128,16]{1,2,0:T(8,128)(2,1)S(1)} %broadcast_in_dim.30), channel_id=1, replica_groups=mesh['dp'=4,'kv_0'=8,'kv_1'=8,'tp'=2] {'tp'}, dimensions={0} | all-to-all | bytes 16384 | tf_op jit(solution)/shard_map/all_to_all | solution.py:23
  173.4 0.1 broadcast_in_dim.32
  173.5 21.7 %all_to_all.66 = bf16[64,128,32]{1,2,0:T(8,128)(2,1)S(1)} all-to-all(bf16[64,128,32]{1,2,0:T(8,128)(2,1)S(1)} %broadcast_in_dim.32), channel_id=1, replica_groups=mesh['dp'=4,'kv_0'=8,'kv_1'=8,'tp'=2] {'kv_0','kv_1'}, dimensions={0} | all-to-all | bytes 1048576 | tf_op jit(solution)/shard_map/all_to_all | solution.py:23
  195.2 0.3 multiply_reduce_fusion
  195.5 0.3 fusion.3
  195.8 0.3 copy-done.4
  196.1 0.2 fusion.45
  196.3 0.5 convolution_convert_fusion.1
  196.9 1.0 copy.35
  197.9 6.3 %all-to-all-start.10 = ((bf16[64,128,32]{1,2,0:T(8,128)(2,1)}), bf16[64,128,32]{1,2,0:T(8,128)(2,1)S(1)}, u32[]{:S(2)}, u32[]{:S(2)}) async-start(bf16[64,128,32]{1,2,0:T(8,128)(2,1)} %bitcast.30), calls=%async_computation.10 | async-start | bytes 1048576 | tf_op jit(solution)/shard_map/all_to_all | solution.py:40
  204.2 0.6 slice.43
  204.8 0.6 fusion.25
  205.4 15.4 %all-to-all-done.10 = bf16[64,128,32]{1,2,0:T(8,128)(2,1)S(1)} async-done(((bf16[64,128,32]{1,2,0:T(8,128)(2,1)}), bf16[64,128,32]{1,2,0:T(8,128)(2,1)S(1)}, u32[]{:S(2)}, u32[]{:S(2)}) %all-to-all-start.10) | async-done | bytes 524320 | tf_op jit(solution)/shard_map/all_to_all | solution.py:40
  220.9 0.1 convert_reduce_fusion.1
  221.0 7.3 %all_to_all.67 = f32[2,128,16]{1,2,0:T(8,128)S(1)} all-to-all(f32[2,128,16]{1,2,0:T(8,128)S(1)} %bitcast.112), channel_id=1, replica_groups=mesh['dp'=4,'kv_0'=8,'kv_1'=8,'tp'=2] {'tp'}, dimensions={0} | all-to-all | bytes 32768 | tf_op jit(solution)/shard_map/all_to_all | solution.py:46
  228.3 0.6 add_convert_fusion
  (74 shorter events, 0.5 us)
Async XLA Ops:
  0.6 40.6 %copy-start = (bf16[44,2048]{1,0:T(8,128)(2,1)S(1)}, bf16[44,2048]{1,0:T(8,128)(2,1)}, u32[]{:S(2)}) copy-start(bf16[44,2048]{1,0:T(8,128)(2,1)} %param.28) | copy-start | bytes 540676
  11.6 28.8 %copy-start.14 = (f32[2048]{0:T(1024)S(1)}, f32[2048]{0:T(1024)}, u32[]{:S(2)}) copy-start(f32[2048]{0:T(1024)} %param.25) | copy-start | bytes 24580
  40.0 0.9 copy-start.3
  40.0 1.2 copy-start.5
  41.7 7.8 %copy-start.12 = (bf16[32,2,256]{2,1,0:T(2,128)(2,1)S(1)}, bf16[32,2,256]{2,1,0:T(2,128)(2,1)}, u32[]{:S(2)}) copy-start(bf16[32,2,256]{2,1,0:T(2,128)(2,1)} %param.32) | copy-start | bytes 98308
  41.7 7.8 %copy-start.18 = (bf16[32,16]{0,1:T(8,128)(2,1)S(1)}, bf16[32,16]{0,1:T(8,128)(2,1)}, u32[]{:S(2)}) copy-start(bf16[32,16]{0,1:T(8,128)(2,1)} %param.33) | copy-start | bytes 3076
  42.8 30.8 %copy-start.13 = (bf16[128,16]{0,1:T(8,128)(2,1)S(1)}, bf16[128,16]{0,1:T(8,128)(2,1)}, u32[]{:S(2)}) copy-start(bf16[128,16]{0,1:T(8,128)(2,1)} %param.24) | copy-start | bytes 12292
  42.8 67.8 %copy-start.8 = (bf16[32,1024]{1,0:T(8,128)(2,1)S(1)}, bf16[32,1024]{1,0:T(8,128)(2,1)}, u32[]{:S(2)}) copy-start(bf16[32,1024]{1,0:T(8,128)(2,1)} %param.31) | copy-start | bytes 196612
  42.8 67.8 %copy-start.9 = (bf16[32,1024]{1,0:T(8,128)(2,1)S(1)}, bf16[32,1024]{1,0:T(8,128)(2,1)}, u32[]{:S(2)}) copy-start(bf16[32,1024]{1,0:T(8,128)(2,1)} %param.30) | copy-start | bytes 196612
  42.8 23.4 %all-to-all-start.2 = ((bf16[64,128,32]{1,2,0:T(8,128)(2,1)}), bf16[64,128,32]{1,2,0:T(8,128)(2,1)S(1)}, u32[]{:S(2)}, u32[]{:S(2)}) async-start(bf16[64,128,32]{1,2,0:T(8,128)(2,1)} %bitcast.9), calls=%async_computation.2 | async-start | bytes 1048576 | tf_op jit(solution)/shard_map/all_to_all | solution.py:40
  74.1 36.4 %all-to-all-start.4 = ((bf16[2,128,16]{1,2,0:T(8,128)(2,1)}), bf16[2,128,16]{1,2,0:T(8,128)(2,1)S(1)}, u32[]{:S(2)}, u32[]{:S(2)}) async-start(bf16[2,128,16]{1,2,0:T(8,128)(2,1)} %broadcast_in_dim.25), calls=%async_computation.4 | async-start | bytes 16384 | tf_op jit(solution)/shard_map/all_to_all | solution.py:23
  111.3 8.8 %copy-start.23 = (f32[16]{0:T(128)S(1)}, f32[16]{0:T(128)}, u32[]{:S(2)}) copy-start(f32[16]{0:T(128)} %param.40) | copy-start | bytes 196
  111.3 8.8 %copy-start.17 = (bf16[2,3,2,256]{3,2,1,0:T(2,128)(2,1)S(1)}, bf16[2,3,2,256]{3,2,1,0:T(2,128)(2,1)}, u32[]{:S(2)}) copy-start(bf16[2,3,2,256]{3,2,1,0:T(2,128)(2,1)} %param.37) | copy-start | bytes 18436
  111.3 8.9 %copy-start.19 = (bf16[4,2,256]{2,1,0:T(2,128)(2,1)S(1)}, bf16[4,2,256]{2,1,0:T(2,128)(2,1)}, u32[]{:S(2)}) copy-start(bf16[4,2,256]{2,1,0:T(2,128)(2,1)} %param.35) | copy-start | bytes 12292
  111.3 8.9 %copy-start.16 = (bf16[4,1024]{1,0:T(4,128)(2,1)S(1)}, bf16[4,1024]{1,0:T(4,128)(2,1)}, u32[]{:S(2)}) copy-start(bf16[4,1024]{1,0:T(4,128)(2,1)} %param.34) | copy-start | bytes 24580
  112.5 28.9 %copy-start.11 = (bf16[2,3,1024]{2,0,1:T(2,128)(2,1)S(1)}, bf16[2,3,1024]{2,0,1:T(2,128)(2,1)}, u32[]{:S(2)}) copy-start(bf16[2,3,1024]{2,0,1:T(2,128)(2,1)} %param.36) | copy-start | bytes 36868
  112.5 29.2 %copy-start.22 = (f32[16]{0:T(128)S(1)}, f32[16]{0:T(128)}, u32[]{:S(2)}) copy-start(f32[16]{0:T(128)} %param.39) | copy-start | bytes 196
  112.5 29.3 %copy-start.2 = (f32[2,16,64,128]{3,2,1,0:T(8,128)S(1)}, f32[2,16,64,128]{3,2,1,0:T(8,128)}, u32[]{:S(2)}) copy-start(f32[2,16,64,128]{3,2,1,0:T(8,128)} %param.38) | copy-start | bytes 3145732
  112.5 28.3 %all-to-all-start.5 = ((bf16[64,2,2576]{2,1,0:T(2,128)(2,1)}), bf16[64,2,2576]{2,1,0:T(2,128)(2,1)S(1)}, u32[]{:S(2)}, u32[]{:S(2)}) async-start(bf16[64,2,2576]{2,1,0:T(2,128)(2,1)} %reshape.103), calls=%async_computation.5 | async-start | bytes 1376256 | tf_op jit(solution)/shard_map/all_to_all | solution.py:40
  142.2 20.7 %copy-start.1 = (f32[2,16,64,128]{3,2,1,0:T(8,128)}, f32[2,16,64,128]{3,2,1,0:T(8,128)S(1)}, u32[]{:S(2)}) copy-start(f32[2,16,64,128]{3,2,1,0:T(8,128)S(1)} %multiply_add_fusion) | copy-start | bytes 3145732
  142.2 0.7 copy-start.21
  142.2 1.1 copy-start.20
  142.2 20.7 %copy-start.10 = (bf16[1024,32]{0,1:T(8,128)(2,1)S(1)}, bf16[1024,32]{0,1:T(8,128)(2,1)}, u32[]{:S(2)}) copy-start(bf16[1024,32]{0,1:T(8,128)(2,1)} %param.43) | copy-start | bytes 196612
  173.4 22.0 %copy-start.15 = (f32[2048]{0:T(1024)S(1)}, f32[2048]{0:T(1024)}, u32[]{:S(2)}) copy-start(f32[2048]{0:T(1024)} %param.44) | copy-start | bytes 24580
  195.2 0.9 copy-start.4
  195.2 1.1 copy-start.6
  195.2 1.2 copy-start.7
  197.9 23.0 %all-to-all-start.10 = ((bf16[64,128,32]{1,2,0:T(8,128)(2,1)}), bf16[64,128,32]{1,2,0:T(8,128)(2,1)S(1)}, u32[]{:S(2)}, u32[]{:S(2)}) async-start(bf16[64,128,32]{1,2,0:T(8,128)(2,1)} %bitcast.30), calls=%async_computation.10 | async-start | bytes 1048576 | tf_op jit(solution)/shard_map/all_to_all | solution.py:40
where the time goes:
time: 230 us; the launch traced here: 229 us
  blocking collectives  137 us (60%)
  waiting for transfers between devices  51.7 us (22%)
  starting transfers between devices  24.3 us (11%)
  local copies, waits for them, and re-layouts  7.9 us (3%)
  other arithmetic  4.19 us (2%)
  matrix products  2.4 us (1%)
    all_to_all x5, blocking collectives, copy_for_each(): lax.all_to_all(jnp.broadcast_to(array[None], (size, *array.shape)), axis,...  83.3 us
    all_to_all x3, waiting for transfers between devices, sum_at_owner(): tiles = lax.all_to_all(cut_along(array, dim, size), axis, 0, 0, tiled=True)  51.7 us
    psum x3, blocking collectives, by_axis(): array = lax.psum(array, axis)  32.8 us
    all_to_all x3, starting transfers between devices, sum_at_owner(): tiles = lax.all_to_all(cut_along(array, dim, size), axis, 0, 0, tiled=True)  20.7 us
    all_to_all x2, blocking collectives, sum_at_owner_2(): lax.all_to_all(tiles, axis, split_axis=0, concat_axis=0, tiled=True)  14.6 us
    all_to_all x1, blocking collectives, sum_at_owner(): tiles = lax.all_to_all(cut_along(array, dim, size), axis, 0, 0, tiled=True)  6.65 us
  transfers between devices with their start and end apart: 4, of which 3 were waited for; matrix products, arithmetic and copies ran while one was open for 1% of the time, Pallas kernels for 0%

commit v1 on v0

v1 whole, which is shorter than its diff:
```python
import jax
import jax.numpy as jnp
from jax import lax
from jax.experimental import pallas as pl
from jax.experimental.pallas import tpu as pltpu
from jax.sharding import Mesh
from jax.sharding import PartitionSpec as P

KV = ("kv_0", "kv_1")
KV_TP = ("kv_0", "kv_1", "tp")
DP_KV = ("dp", "kv_0", "kv_1")
EPS = 1e-06
MESH = pl.DeviceIdType.MESH
BF = jnp.bfloat16
F32 = jnp.float32
FAR_FIRST = (4, 5, 3, 6, 2, 7, 1)
NEAR_FIRST = (1, 7, 2, 6, 3, 5, 4)
HID = 44
WIDE = 2688


def dot(a, b, ca, cb):
    return lax.dot_general(a, b, (((ca,), (cb,)), ((), ())), preferred_element_type=F32)


def silu(v):
    return v * (1.0 / (1.0 + jnp.exp(-v)))


def iota(shape, dim):
    return lax.broadcasted_iota(jnp.int32, shape, dim)


def kernel(
    tokens_h, gate1_h, up1_h, down1_h, gain1_h, proj_z_h, proj_x_h, proj_bc_h, proj_dt_h, gain_m_h, conv_x_h, conv_bc_h,
    win_x_h, win_bc_h, dt_bias_h, log_rate_h, skip_gain_h, group_gain_h, state_h, out_h, gate2_h, up2_h, down2_h, gain2_h,
    result_o, state_o, win_x_o, win_bc_o,
    gate1, up1, down1, gain1, proj_z, proj_x, proj_bc_raw, proj_dt, gain_m, conv_x_raw, conv_bc_raw,
    win_x_raw, win_bc_raw, dt_bias, log_rate, skip_gain, group_gain, state, out_w, gate2, up2, down2, gain2,
    proj_bc, conv_x, conv_bc, win_x, win_bc, new_state, new_win_x, new_win_bc, result_v,
    wt1, wd1, wt2, wd2, xt1, xt2, pair_out1, pair_in1, pair_out2, pair_in2,
    s1, s2, ra1, ra2, t1, t2, rb1, rb2, af, proj_s, proj_r, quad, quad_b, quad_r,
    mix_a, mix_f, mix_x, out_s, out_r,
    load_sem, local_sem, ssem, rsem, psem, qsem,
):
    z, y, t = lax.axis_index("kv_0"), lax.axis_index("kv_1"), lax.axis_index("tp")
    u = 1 - t
    a = z * u + y * t
    b = y * u + z * t

    def ring_a(i):
        return {"kv_0": lax.rem(z + u * i, 8), "kv_1": lax.rem(y + t * i, 8)}

    def ring_b(i):
        return {"kv_0": lax.rem(z + t * i, 8), "kv_1": lax.rem(y + u * i, 8)}

    def ring_z(i):
        return {"kv_0": lax.rem(z + i, 8)}

    def ring_y(i):
        return {"kv_1": lax.rem(y + i, 8)}

    partner = {"tp": u}

    def remote(src, dst, send, recv, peer):
        return pltpu.make_async_remote_copy(
            src_ref=src, dst_ref=dst, send_sem=send, recv_sem=recv, device_id=peer, device_id_type=MESH
        )

    barrier = pltpu.get_barrier_semaphore()
    for i in range(1, 8):
        pl.semaphore_signal(barrier, 1, device_id=ring_z(i), device_id_type=MESH)
        pl.semaphore_signal(barrier, 1, device_id=ring_y(i), device_id_type=MESH)
    pl.semaphore_signal(barrier, 1, device_id=partner, device_id_type=MESH)

    loads = [
        pltpu.make_async_copy(src, dst, load_sem.at[n])
        for n, (src, dst) in enumerate(
            [
                (tokens_h, xt1.at[z, y, t]), (gate1_h, gate1), (up1_h, up1), (down1_h, down1), (gain1_h, gain1),
                (proj_z_h, proj_z), (proj_x_h, proj_x), (proj_bc_h, proj_bc_raw), (proj_dt_h, proj_dt), (gain_m_h, gain_m),
                (conv_x_h, conv_x_raw), (conv_bc_h, conv_bc_raw), (win_x_h, win_x_raw), (win_bc_h, win_bc_raw),
                (dt_bias_h, dt_bias), (log_rate_h, log_rate), (skip_gain_h, skip_gain), (group_gain_h, group_gain),
                (state_h, state), (out_h, out_w),
                (gate2_h, gate2), (up2_h, up2), (down2_h, down2), (gain2_h, gain2),
            ]
        )
    ]
    for load in loads:
        load.start()

    eye = (iota((128, 128), 0) == iota((128, 128), 1)).astype(BF)
    row = iota((128, 128), 0)
    col = iota((128, 128), 1)
    swapped = ((row >> 1) & 7) * 16 + (row >> 4) * 2 + (row & 1)
    perm = (jnp.where(t == 0, row, swapped) == col).astype(BF)

    def prepare(gate, up, down, gain, wt, wd):
        for r in range(16):
            rows = pl.ds(128 * r, 128)
            g = gain[:, rows]
            wt[0, :, rows] = (gate[:, rows].astype(F32) * g).astype(BF)
            wt[1, :, rows] = (up[:, rows].astype(F32) * g).astype(BF)
            wd[rows, :] = dot(down[:, rows], eye[:HID, :HID], 0, 0).astype(BF)

    def gather_features(ph, xt, block, work=None):
        if block is not None:
            xt[z, y, t] = block

        def first(core):
            def go():
                peers = ring_y if core == 0 else ring_z
                own = xt.at[z, y, core]
                for i in FAR_FIRST:
                    remote(own, own, ssem.at[ph, i], rsem.at[ph, i], peers(i)).start()

            return go

        def second(core):
            def go():
                peers, across = (ring_y, ring_z) if core == 0 else (ring_z, ring_y)
                own = xt.at[z, y, core]

                def line(k):
                    return xt.at[lax.rem(z + k, 8), :, core] if core == 0 else xt.at[:, lax.rem(y + k, 8), core]

                for i in NEAR_FIRST:
                    remote(own, own, ssem.at[ph, i], rsem.at[ph, i], peers(i)).wait()
                mine = line(0)
                for i in FAR_FIRST:
                    remote(mine, mine, ssem.at[ph + 1, i], rsem.at[ph + 1, i], across(i)).start()
                remote(mine, mine, psem.at[ph, 0], qsem.at[ph, 0], partner).start()
                for i in NEAR_FIRST:
                    remote(mine, mine, ssem.at[ph + 1, i], rsem.at[ph + 1, i], across(i)).wait()
                    other = line(8 - i)
                    remote(other, other, psem.at[ph, i], qsem.at[ph, i], partner).start()
                for i in range(8):
                    remote(mine, mine, psem.at[ph, i], qsem.at[ph, i], partner).wait()

            return go

        pl.when(t == 0)(first(0))
        pl.when(t == 1)(first(1))
        if work is not None:
            work()
        pl.when(t == 0)(second(0))
        pl.when(t == 1)(second(1))

    def mlp(ph, xt, wt, wd, pair_out, pair_in, s, ra, tb, rb):
        x = xt[...].reshape(2048, 128)
        xf = x.astype(F32)
        factor = lax.rsqrt(jnp.sum(xf * xf, axis=0, keepdims=True) * (1.0 / 2048) + EPS)
        gate = dot(wt[0], x, 1, 0) * factor
        up = dot(wt[1], x, 1, 0) * factor
        hidden = (silu(gate) * up).astype(BF)
        for k in range(8):
            part = dot(wd[pl.ds(256 * k, 256), :], hidden, 1, 0).astype(BF)
            pair_out[k] = part.reshape(8, 2, 16, 128)
            remote(pair_out.at[k, :, u], pair_in.at[k], psem.at[ph, k], qsem.at[ph, k], partner).start()
        for k in range(8):
            remote(pair_out.at[k, :, u], pair_in.at[k], psem.at[ph, k], qsem.at[ph, k], partner).wait()
            for m in range(8):
                total = pair_out[k, m, t].astype(F32) + pair_in[k, m].astype(F32)
                s[k * u + m * t, m * u + k * t] = total.astype(BF)
        for i in FAR_FIRST:
            remote(s.at[lax.rem(a + i, 8)], ra.at[a], ssem.at[ph, i], rsem.at[ph, i], ring_a(i)).start()
        total = s[a].astype(F32)
        for i in NEAR_FIRST:
            remote(s.at[lax.rem(a + i, 8)], ra.at[a], ssem.at[ph, i], rsem.at[ph, i], ring_a(i)).wait()
            total = total + ra[lax.rem(a + 8 - i, 8)].astype(F32)
        tb[...] = total.astype(BF)
        for i in FAR_FIRST:
            remote(tb.at[lax.rem(b + i, 8)], rb.at[b], ssem.at[ph + 1, i], rsem.at[ph + 1, i], ring_b(i)).start()
        total = tb[b].astype(F32)
        for i in NEAR_FIRST:
            remote(tb.at[lax.rem(b + i, 8)], rb.at[b], ssem.at[ph + 1, i], rsem.at[ph + 1, i], ring_b(i)).wait()
            total = total + rb[lax.rem(b + 8 - i, 8)].astype(F32)
        return total

    loads[0].wait()
    pl.semaphore_wait(barrier, 15)

    def work1():
        for load in loads[1:18]:
            load.wait()
        prepare(gate1, up1, down1, gain1, wt1, wd1)
        raw = proj_bc_raw[...].astype(F32)
        proj_bc[:, :256] = raw[:, 0].astype(BF)
        proj_bc[:, 256:] = raw[:, 1].astype(BF)
        taps = conv_x_raw[...].astype(F32)
        for k in range(8):
            lanes = slice(128 * k, 128 * k + 128)
            conv_x[:, k, :] = taps[:, lanes]
            for j in range(3):
                win_x[:, j, k, :] = win_x_raw[j].astype(F32)[:, lanes]
        taps = conv_bc_raw[...].astype(F32)
        window = win_bc_raw[...].astype(F32)
        for k in range(4):
            lanes = slice(128 * (k % 2), 128 * (k % 2) + 128)
            conv_bc[:, k, :] = taps[:, k // 2, lanes]
            win_bc[:, :, k, :] = window[:, :, k // 2, lanes]

    gather_features(0, xt1, None, work1)
    tokens_t = xt1[z, y, t].astype(F32)
    sum1 = mlp(2, xt1, wt1, wd1, pair_out1, pair_in1, s1, ra1, t1, rb1)
    first = (tokens_t + 0.5 * sum1).astype(BF)

    af[t] = first
    swap = remote(af.at[t], af.at[t], psem.at[4, 0], qsem.at[4, 0], partner)
    swap.start()
    kv = z * 8 + y
    gains = gain_m[pl.ds(kv // 4, 1), :]
    lane0 = lax.rem(kv, 4)
    gain32 = jnp.where(
        lane0 < 2,
        jnp.where(lane0 == 0, gains[:, :32], gains[:, 32:64]),
        jnp.where(lane0 == 2, gains[:, 64:96], gains[:, 96:]),
    )
    swap.wait()
    rows32 = dot(perm, af[...].reshape(32, 128), 1, 1)
    squares = jnp.sum(rows32 * rows32, axis=1, keepdims=True)
    left = (rows32 * gain32).astype(BF)

    def put(start, value):
        width = value.shape[1]
        proj_s[:, :, pl.ds(start, width)] = value.astype(BF).reshape(8, 16, width)

    put(0, dot(left, proj_z[...], 1, 0))
    put(1024, dot(left, proj_x[...], 1, 0))
    put(2048, dot(left, proj_bc[...], 1, 0))
    last = jnp.concatenate([dot(left, proj_dt[...], 1, 1), squares, jnp.zeros((128, 111), F32)], axis=1)
    put(2560, last)
    for i in FAR_FIRST:
        remote(proj_s.at[lax.rem(a + i, 8)], proj_r.at[a], ssem.at[4, i], rsem.at[4, i], ring_a(i)).start()
    loads[18].wait()
    for i in NEAR_FIRST:
        remote(proj_s.at[lax.rem(a + i, 8)], proj_r.at[a], ssem.at[4, i], rsem.at[4, i], ring_a(i)).wait()
    for k in range(21):
        lanes = pl.ds(128 * k, 128)
        total = proj_s[a, :, lanes].astype(F32)
        for i in NEAR_FIRST:
            total = total + proj_r[lax.rem(a + 8 - i, 8), :, lanes].astype(F32)
        quad[:, k, :] = total
    quad[:, 21:24, :] = jnp.zeros((16, 3, 128), F32)
    quad_b[:, :24, :] = quad[...].astype(BF)
    quad_b[:, 24:, :] = jnp.zeros((16, 8, 128), BF)
    for i in FAR_FIRST:
        remote(
            quad_b.at[pl.ds(2 * lax.rem(b + i, 8), 2)], quad_r.at[b], ssem.at[5, i], rsem.at[5, i], ring_b(i)
        ).start()
    full = quad[pl.ds(2 * b, 2)]
    for i in NEAR_FIRST:
        remote(
            quad_b.at[pl.ds(2 * lax.rem(b + i, 8), 2)], quad_r.at[b], ssem.at[5, i], rsem.at[5, i], ring_b(i)
        ).wait()
        full = full + quad_r[lax.rem(b + 8 - i, 8)].astype(F32)[:, :24, :]

    head_of_row = iota((8, 16), 0)
    head = iota((8, 16), 1)
    lane = iota((8, 128), 1)
    even, odd = head == 2 * head_of_row, head == 2 * head_of_row + 1

    def per_channel(v):
        low = jnp.sum(jnp.where(even, v, 0.0), axis=1, keepdims=True)
        high = jnp.sum(jnp.where(odd, v, 0.0), axis=1, keepdims=True)
        return jnp.where(lane < 64, low, high)

    skip = per_channel(skip_gain[...])
    lane_sq = iota((128, 128), 1)
    contracted = jnp.zeros((128, 128), F32)
    kept, news = [], []
    for s in range(2):
        both = full[s]
        factor = lax.rsqrt(both[20:21, 16:17] * (1.0 / 2048) + EPS)
        both = both * factor
        gate_z = both[0:8].astype(BF).astype(F32)
        x_new = both[8:16].astype(BF).astype(F32)
        bc_new = both[16:20].astype(BF).astype(F32)
        rate = both[20:21, :16] + dt_bias[...]
        conv = x_new * conv_x[3]
        conv2 = bc_new * conv_bc[3]
        for j in range(3):
            conv = conv + win_x[s, j] * conv_x[j]
            conv2 = conv2 + win_bc[s, j] * conv_bc[j]
        x_in = silu(conv)
        bc_in = silu(conv2)
        step = jnp.maximum(rate, 0.0) + jnp.log1p(jnp.exp(-jnp.abs(rate)))
        retain = jnp.exp(-step * jnp.exp(log_rate[...]))
        sx = per_channel(step) * x_in
        news.append((x_new, bc_new))
        for k in range(8):
            c = bc_in[2 + k // 4 : 3 + k // 4]
            column = jnp.sum(state[s, k] * c, axis=1, keepdims=True)
            contracted = jnp.where(lane_sq == s * 8 + k, column, contracted)
        kept.append((gate_z, x_in, bc_in, per_channel(retain), sx))
    rows = contracted.T
    blocks = []
    for s in range(2):
        gate_z, x_in, bc_in, retain, sx = kept[s]
        dots = jnp.sum(bc_in[0:2] * bc_in[2:4], axis=1, keepdims=True)
        group = iota((8, 128), 0) < 4
        bdotc = jnp.where(group, dots[0:1], dots[1:2])
        readout = retain * rows[8 * s : 8 * s + 8] + sx * bdotc + skip * x_in
        gated = readout * silu(gate_z)
        sq = jnp.sum(gated * gated, axis=1, keepdims=True)
        low = jnp.sum(sq[0:4], axis=0, keepdims=True)
        high = jnp.sum(sq[4:8], axis=0, keepdims=True)
        scale = lax.rsqrt(jnp.where(group, low, high) * (1.0 / 512) + EPS)
        blocks.append(gated * scale * group_gain[...])
    mixed = jnp.concatenate(blocks, axis=0).astype(BF)

    mix_a[b] = mixed
    for i in FAR_FIRST:
        remote(mix_a.at[b], mix_a.at[b], ssem.at[6, i], rsem.at[6, i], ring_b(i)).start()
    for load in loads[19:]:
        load.wait()
    prepare(gate2, up2, down2, gain2, wt2, wd2)
    packed = jnp.concatenate([kept[0][3], kept[1][3], kept[0][4], kept[1][4]], axis=0).T
    for s in range(2):
        for k in range(8):
            j = 8 * s + k
            bvec = kept[s][2][k // 4 : k // 4 + 1]
            new_state[s, k] = packed[:, j : j + 1] * state[s, k] + packed[:, 16 + j : 17 + j] * bvec
        new_win_bc[s, 0:2] = win_bc_raw[s, 1:3]
        for c in range(2):
            bc_new = news[s][1]
            line = jnp.concatenate([bc_new[2 * c : 2 * c + 1], bc_new[2 * c + 1 : 2 * c + 2]], axis=1)
            new_win_bc[s, 2, c : c + 1, :] = line.astype(BF)
    new_win_x[0] = win_x_raw[1]
    new_win_x[1] = win_x_raw[2]
    lines = [jnp.concatenate([news[s][0][k : k + 1] for k in range(8)], axis=1) for s in range(2)]
    new_win_x[2] = jnp.concatenate(lines, axis=0).astype(BF)
    stores = [
        pltpu.make_async_copy(src, dst, local_sem.at[n])
        for n, (src, dst) in enumerate([(new_state, state_o), (new_win_x, win_x_o), (new_win_bc, win_bc_o)])
    ]
    for store in stores:
        store.start()
    for i in NEAR_FIRST:
        remote(mix_a.at[b], mix_a.at[b], ssem.at[6, i], rsem.at[6, i], ring_b(i)).wait()
    mix_f[...] = mix_a[...].reshape(128, 128).astype(F32)
    for k in range(8):
        mix_x[a, :, pl.ds(128 * k, 128)] = mix_f[pl.ds(k, 16, stride=8), :].astype(BF)
    for i in FAR_FIRST:
        remote(mix_x.at[a], mix_x.at[a], ssem.at[7, i], rsem.at[7, i], ring_a(i)).start()
    for i in NEAR_FIRST:
        remote(mix_x.at[a], mix_x.at[a], ssem.at[7, i], rsem.at[7, i], ring_a(i)).wait()
    partial = dot(out_w[...], mix_x[...].reshape(128, 1024), 1, 1).astype(BF)
    halves = dot(partial, perm, 1, 0)
    out_s[...] = halves.astype(BF).reshape(2, 16, 128)
    swap = remote(out_s.at[u], out_r, psem.at[5, 0], qsem.at[5, 0], partner)
    swap.start()
    swap.wait()
    mixed_sum = out_s[t].astype(F32) + out_r[...].astype(F32)
    after = (first.astype(F32) + mixed_sum).astype(BF)

    gather_features(8, xt2, after)
    sum2 = mlp(10, xt2, wt2, wd2, pair_out2, pair_in2, s2, ra2, t2, rb2)
    result_v[...] = (after.astype(F32) + 0.5 * sum2).astype(BF)
    stores.append(pltpu.make_async_copy(result_v, result_o, local_sem.at[3]))
    stores[3].start()
    for store in stores:
        store.wait()


def per_device(
    tokens, mlp1_gain, mlp1_gate, mlp1_up, mlp1_down, mixer_gain, proj_z, proj_x, proj_bc, proj_dt, conv_x, conv_bc,
    window_x, window_bc, ssm_state, dt_bias, log_rate, skip_gain, group_gain, out_weight, mlp2_gain, mlp2_gate,
    mlp2_up, mlp2_down,
):
    hbm = pl.BlockSpec(memory_space=pltpu.HBM)
    sds = jax.ShapeDtypeStruct
    inputs = [
        tokens.T, mlp1_gate.T, mlp1_up.T, mlp1_down, mlp1_gain.reshape(1, 2048), proj_z, proj_x, proj_bc, proj_dt.T,
        mixer_gain.reshape(16, 128), conv_x, conv_bc, window_x.transpose(1, 0, 2), window_bc, dt_bias.reshape(1, 16),
        log_rate.reshape(1, 16), skip_gain.reshape(1, 16), group_gain.reshape(8, 128), ssm_state.reshape(2, 8, 128, 128),
        out_weight.T, mlp2_gate.T, mlp2_up.T, mlp2_down, mlp2_gain.reshape(1, 2048),
    ]
    outs = [sds((16, 128), BF), sds((2, 8, 128, 128), F32), sds((3, 2, 1024), BF), sds((2, 3, 2, 256), BF)]
    dma = pltpu.SemaphoreType.DMA
    tile = (16, 128)
    scratch = [pltpu.VMEM(v.shape, v.dtype) for v in inputs[1:]]
    scratch += [
        pltpu.VMEM((32, 512), BF), pltpu.VMEM((4, 8, 128), F32), pltpu.VMEM((4, 4, 128), F32),
        pltpu.VMEM((2, 3, 8, 128), F32), pltpu.VMEM((2, 3, 4, 128), F32),
        pltpu.VMEM((2, 8, 128, 128), F32), pltpu.VMEM((3, 2, 1024), BF), pltpu.VMEM((2, 3, 2, 256), BF),
        pltpu.VMEM((16, 128), BF),
        pltpu.VMEM((2, HID, 2048), BF), pltpu.VMEM((2048, HID), BF),
        pltpu.VMEM((2, HID, 2048), BF), pltpu.VMEM((2048, HID), BF),
        pltpu.VMEM((8, 8, 2, *tile), BF), pltpu.VMEM((8, 8, 2, *tile), BF),
        pltpu.VMEM((8, 8, 2, *tile), BF), pltpu.VMEM((8, 8, *tile), BF),
        pltpu.VMEM((8, 8, 2, *tile), BF), pltpu.VMEM((8, 8, *tile), BF),
        pltpu.VMEM((8, 8, *tile), BF), pltpu.VMEM((8, 8, *tile), BF),
        pltpu.VMEM((8, 8, *tile), BF), pltpu.VMEM((8, 8, *tile), BF),
        pltpu.VMEM((8, *tile), BF), pltpu.VMEM((8, *tile), BF),
        pltpu.VMEM((8, *tile), BF), pltpu.VMEM((8, *tile), BF),
        pltpu.VMEM((2, *tile), BF),
        pltpu.VMEM((8, 16, WIDE), BF), pltpu.VMEM((8, 16, WIDE), BF),
        pltpu.VMEM((16, 24, 128), F32), pltpu.VMEM((16, 32, 128), BF), pltpu.VMEM((8, 2, 32, 128), BF),
        pltpu.VMEM((8, *tile), BF), pltpu.VMEM((128, 128), F32), pltpu.VMEM((8, 16, 1024), BF),
        pltpu.VMEM((2, *tile), BF), pltpu.VMEM(tile, BF),
        dma((24,)), dma((4,)), dma((12, 8)), dma((12, 8)), dma((12, 8)), dma((12, 8)),
    ]
    result, new_state, new_x, new_bc = pl.pallas_call(
        kernel,
        out_shape=outs,
        in_specs=[hbm] * len(inputs),
        out_specs=[hbm] * len(outs),
        scratch_shapes=scratch,
        compiler_params=pltpu.CompilerParams(
            collective_id=1, has_side_effects=True, vmem_limit_bytes=67043328
        ),
    )(*inputs)
    return (result.T, new_state.reshape(2, 16, 64, 128), new_x.transpose(1, 0, 2), new_bc)


def solution(mesh):
    torus = Mesh(
        mesh.devices.reshape(mesh.shape["dp"], 8, 8, mesh.shape["tp"]), ("dp", "kv_0", "kv_1", "tp")
    )
    placed = (
        P("dp", KV_TP),
        P(),
        P(None, KV_TP),
        P(None, KV_TP),
        P(KV_TP, None),
        P(),
        P(KV, "tp"),
        P(KV, "tp"),
        P(KV, None, "tp"),
        P(KV, "tp"),
        P(None, "tp"),
        P(None, None, "tp"),
        P(DP_KV, None, "tp"),
        P(DP_KV, None, None, "tp"),
        P(DP_KV, "tp", None, None),
        P("tp"),
        P("tp"),
        P("tp"),
        P("tp"),
        P("tp", KV),
        P(),
        P(None, KV_TP),
        P(None, KV_TP),
        P(KV_TP, None),
    )
    return jax.shard_map(
        per_device,
        mesh=torus,
        in_specs=placed,
        out_specs=(
            P("dp", KV_TP),
            P(DP_KV, "tp", None, None),
            P(DP_KV, None, "tp"),
            P(DP_KV, None, None, "tp"),
        ),
        check_vma=False,
    )
```

time: 230 us -> 102 us (0.44)
  blocking collectives: 137 us -> 0 us
  Pallas kernels: 0 us -> 96.4 us
  waiting for transfers between devices: 51.7 us -> 0 us
  starting transfers between devices: 24.3 us -> 0 us
  other arithmetic: 4.19 us -> 0 us
  local copies, waits for them, and re-layouts: 7.9 us -> 4.87 us
  matrix products: 2.4 us -> 0 us
    all_to_all x8 -> x0, blocking collectives: 105 us -> none  [the longest x5 83.3 us: copy_for_each(): lax.all_to_all(jnp.broadcast_to(array[None], (size, *array.shape)), axis,...]
    pallas_call x0 -> x1, Pallas kernels: none -> 96.4 us  [per_device(): pl.pallas_call(kernel, out_shape=outs, in_specs=[hbm] * len(inputs), out_...]
    all_to_all x4 -> x0, waiting for transfers between devices: 51.7 us -> none  [the longest x3 51.7 us: sum_at_owner(): tiles = lax.all_to_all(cut_along(array, dim, size), axis, 0, 0, tiled=True)]
    psum x3 -> x0, blocking collectives: 32.8 us -> none  [by_axis(): array = lax.psum(array, axis)]
    all_to_all x4 -> x0, starting transfers between devices: 24.3 us -> none  [the longest x3 20.7 us: sum_at_owner(): tiles = lax.all_to_all(cut_along(array, dim, size), axis, 0, 0, tiled=True)]
    unnamed x53 -> x10, local copies, waits for them, and re-layouts: 1.12 us -> 4.87 us
    dot_general x7 -> x0, matrix products: 2.4 us -> none  [the longest x2 1.05 us: half_mlp(): jnp.dot(hidden, down_weight, preferred_element_type=jnp.float32)]
    convert_element_type x3 -> x0, local copies, waits for them, and re-layouts: 2.34 us -> none  [the longest x2 2 us: half_mlp(): paired_sums = sum_at_owner(partial_sums.astype(jnp.bfloat16), KV, 1)]
  transfers between devices with their start and end apart: 4 -> 0, of which waited for: 3 -> 0; matrix products, arithmetic and copies ran while one was open for 1% -> 0% of each run, Pallas kernels for 0% -> 0%
where the time goes in v1:
time: 102 us
  Pallas kernels  96.4 us (95%)
  local copies, waits for them, and re-layouts  4.87 us (5%)
    pallas_call x1, Pallas kernels, per_device(): pl.pallas_call(kernel, out_shape=outs, in_specs=[hbm] * len(inputs), out_...  96.4 us
    unnamed x10, local copies, waits for them, and re-layouts  4.87 us

profile of v1, /device:TPU:1, one launch (start us, length us, event | category | flops | bytes accessed | tf_op | source)
XLA Modules:
  0.0 101.9 jit_solution(10744276831954042820)
XLA Ops:
  0.6 96.4 %shard_map.255 = (bf16[16,128]{1,0:T(8,128)(2,1)}, f32[2,8,128,128]{3,2,1,0:T(8,128)}, bf16[3,2,1024]{2,1,0:T(2,128)(2,1)}, bf16[2,3,2,256]{3,2,1,0:T(2,128)(2,1)}) custom-call(bf16[16,128]{1,0:T(8,128)(2,1)} %bitcast.31, bf16[44,2048]{1,0:T(8,128)(2,1)} %bitcast.21, bf16[44,2048]{1,0:T(8,128)(2,1)} %bitcast.22, bf16[44,2048]{1,0:T(8,128)(2,1)} %down1_h.1, ...), custom_call_target="tpu_custom_call" | custom-call | tf_op jit(solution)/shard_map/pallas_call | solution.py:404
  97.0 0.0 copy-start.2
  97.1 0.7 copy-done.2
  97.7 0.6 copy.32
  98.3 0.0 copy-start
  98.3 2.3 %copy.33 = f32[2,16,64,128]{3,2,1,0:T(8,128)} copy(f32[2,16,64,128]{3,2,1,0:T(8,128)} %bitcast.20) | data formatting | bytes 2097152
  100.6 0.0 copy-done
  100.6 0.0 copy-start.1
  100.6 0.6 copy.34
  101.2 0.1 copy-done.1
  101.3 0.6 copy.35
Async XLA Ops:
  97.0 0.7 copy-start.2
  98.3 2.3 %copy-start = (bf16[3,2,1024]{2,1,0:T(2,128)(2,1)S(1)}, bf16[3,2,1024]{2,1,0:T(2,128)(2,1)}, u32[]{:S(2)}) copy-start(bf16[3,2,1024]{2,1,0:T(2,128)(2,1)} %get-tuple-element.10) | copy-start | bytes 36868
  100.6 0.7 copy-start.1

commit v2 on v1

--- a/solution.py
+++ b/solution.py
@@ -15,6 +15,7 @@
 F32 = jnp.float32
 FAR_FIRST = (4, 5, 3, 6, 2, 7, 1)
 NEAR_FIRST = (1, 7, 2, 6, 3, 5, 4)
+FAR, NEAR = (4, 5, 3), (6, 2, 7, 1)
 HID = 44
 WIDE = 2688
 
@@ -40,8 +41,8 @@
     proj_bc, conv_x, conv_bc, win_x, win_bc, new_state, new_win_x, new_win_bc, result_v,
     wt1, wd1, wt2, wd2, xt1, xt2, pair_out1, pair_in1, pair_out2, pair_in2,
     s1, s2, ra1, ra2, t1, t2, rb1, rb2, af, proj_s, proj_r, quad, quad_b, quad_r,
-    mix_a, mix_f, mix_x, out_s, out_r,
-    load_sem, local_sem, ssem, rsem, psem, qsem,
+    mix_a, mix_f, af_q, out_s, out_r,
+    load_sem, local_sem, ssem, rsem, psem, qsem, gsem, wsem, vsem,
 ):
     z, y, t = lax.axis_index("kv_0"), lax.axis_index("kv_1"), lax.axis_index("tp")
     u = 1 - t
@@ -66,6 +67,20 @@
         return pltpu.make_async_remote_copy(
             src_ref=src, dst_ref=dst, send_sem=send, recv_sem=recv, device_id=peer, device_id_type=MESH
         )
+
+    def relay(step):
+        for way in (0, 1) if step < 4 else (0,):
+            shift = 1 if way == 0 else 7
+            if step > 1:
+                back = lax.rem(y + (8 - step + 1) * shift, 8)
+                remote(out_w.at[back], out_w.at[back], wsem.at[way, step - 1], vsem.at[way, step - 1], ring_y(shift)).wait()
+            if step <= (4 if way == 0 else 3):
+                block = out_w.at[lax.rem(y + (8 - step + 1) * shift, 8)]
+                remote(block, block, wsem.at[way, step], vsem.at[way, step], ring_y(shift)).start()
+
+    def relay_end():
+        for way, step in ((0, 4), (1, 3)):
+            remote(out_w.at[0], out_w.at[0], wsem.at[way, step], vsem.at[way, step], ring_y(1)).wait()
 
     barrier = pltpu.get_barrier_semaphore()
     for i in range(1, 8):
@@ -81,7 +96,7 @@
                 (proj_z_h, proj_z), (proj_x_h, proj_x), (proj_bc_h, proj_bc_raw), (proj_dt_h, proj_dt), (gain_m_h, gain_m),
                 (conv_x_h, conv_x_raw), (conv_bc_h, conv_bc_raw), (win_x_h, win_x_raw), (win_bc_h, win_bc_raw),
                 (dt_bias_h, dt_bias), (log_rate_h, log_rate), (skip_gain_h, skip_gain), (group_gain_h, group_gain),
-                (state_h, state), (out_h, out_w),
+                (state_h, state), (out_h, out_w.at[y]),
                 (gate2_h, gate2), (up2_h, up2), (down2_h, down2), (gain2_h, gain2),
             ]
         )
@@ -101,41 +116,58 @@
             g = gain[:, rows]
             wt[0, :, rows] = (gate[:, rows].astype(F32) * g).astype(BF)
             wt[1, :, rows] = (up[:, rows].astype(F32) * g).astype(BF)
-            wd[rows, :] = dot(down[:, rows], eye[:HID, :HID], 0, 0).astype(BF)
-
-    def gather_features(ph, xt, block, work=None):
+            turned = dot(down[:, rows], eye[:HID, :HID], 0, 0).astype(BF)
+            wd[r // 2, pl.ds(4 * (r % 2), 4)] = turned.reshape(4, 2, 16, HID)
+
+    def gather_features(g, xt, block, work=None):
         if block is not None:
             xt[z, y, t] = block
+        sa, ra_, sb, rb_, sp, rp = (gsem.at[g, n] for n in range(6))
+
+        def parts(core):
+            peers, across = (ring_y, ring_z) if core == 0 else (ring_z, ring_y)
+
+            def cell(k):
+                return xt.at[z, lax.rem(y + k, 8), core] if core == 0 else xt.at[lax.rem(z + k, 8), y, core]
+
+            def line(k):
+                return xt.at[:, lax.rem(y + k, 8), core] if core == 0 else xt.at[lax.rem(z + k, 8), :, core]
+
+            seven = xt.at[pl.ds(0, 7), 0, core] if core == 0 else xt.at[0, pl.ds(0, 7), core]
+
+            def onward(k, distances):
+                src = cell(8 - k)
+                for i in distances:
+                    remote(src, src, sb.at[k], rb_.at[k], across(i)).start()
+
+            return peers, across, cell, line, seven, onward
 
         def first(core):
             def go():
-                peers = ring_y if core == 0 else ring_z
-                own = xt.at[z, y, core]
+                peers, _, cell, _, _, onward = parts(core)
+                own = cell(0)
                 for i in FAR_FIRST:
-                    remote(own, own, ssem.at[ph, i], rsem.at[ph, i], peers(i)).start()
+                    remote(own, own, sa.at[i], ra_.at[i], peers(i)).start()
+                onward(0, FAR_FIRST)
 
             return go
 
         def second(core):
             def go():
-                peers, across = (ring_y, ring_z) if core == 0 else (ring_z, ring_y)
-                own = xt.at[z, y, core]
-
-                def line(k):
-                    return xt.at[lax.rem(z + k, 8), :, core] if core == 0 else xt.at[:, lax.rem(y + k, 8), core]
-
+                peers, across, cell, line, seven, onward = parts(core)
+                own = cell(0)
                 for i in NEAR_FIRST:
-                    remote(own, own, ssem.at[ph, i], rsem.at[ph, i], peers(i)).wait()
-                mine = line(0)
-                for i in FAR_FIRST:
-                    remote(mine, mine, ssem.at[ph + 1, i], rsem.at[ph + 1, i], across(i)).start()
-                remote(mine, mine, psem.at[ph, 0], qsem.at[ph, 0], partner).start()
+                    remote(own, own, sa.at[i], ra_.at[i], peers(i)).wait()
+                    onward(i, FAR)
                 for i in NEAR_FIRST:
-                    remote(mine, mine, ssem.at[ph + 1, i], rsem.at[ph + 1, i], across(i)).wait()
-                    other = line(8 - i)
-                    remote(other, other, psem.at[ph, i], qsem.at[ph, i], partner).start()
-                for i in range(8):
-                    remote(mine, mine, psem.at[ph, i], qsem.at[ph, i], partner).wait()
+                    onward(i, NEAR)
+                for k in (0, *NEAR_FIRST):
+                    remote(seven, seven, sb.at[k], rb_.at[k], across(1)).wait()
+                    src = line(8 - k)
+                    remote(src, src, sp.at[k], rp.at[k], partner).start()
+                for k in range(8):
+                    src = line(0)
+                    remote(src, src, sp.at[k], rp.at[k], partner).wait()
 
             return go
 
@@ -146,36 +178,57 @@
         pl.when(t == 0)(second(0))
         pl.when(t == 1)(second(1))
 
-    def mlp(ph, xt, wt, wd, pair_out, pair_in, s, ra, tb, rb):
-        x = xt[...].reshape(2048, 128)
-        xf = x.astype(F32)
-        factor = lax.rsqrt(jnp.sum(xf * xf, axis=0, keepdims=True) * (1.0 / 2048) + EPS)
-        gate = dot(wt[0], x, 1, 0) * factor
-        up = dot(wt[1], x, 1, 0) * factor
+    def mlp(g, xt, wt, wd, pair_out, pair_in, sums, ra, tb, rb):
+        if g == 1:
+            x, cx = xt[...].reshape(2048, 128), 0
+            xf = x.astype(F32)
+            squares = jnp.sum(xf * xf, axis=0, keepdims=True)
+        else:
+            x = jnp.concatenate([xt[k // 2, :, k % 2].reshape(128, 128) for k in range(16)], axis=1)
+            cx = 1
+            xf = x.astype(F32)
+            squares = dot(jnp.ones((8, 2048), BF), (xf * xf).astype(BF), 1, 1)[0:1]
+        factor = lax.rsqrt(squares * (1.0 / 2048) + EPS)
+        gate = dot(wt[0], x, 1, cx) * factor
+        up = dot(wt[1], x, 1, cx) * factor
         hidden = (silu(gate) * up).astype(BF)
-        for k in range(8):
-            part = dot(wd[pl.ds(256 * k, 256), :], hidden, 1, 0).astype(BF)
-            pair_out[k] = part.reshape(8, 2, 16, 128)
-            remote(pair_out.at[k, :, u], pair_in.at[k], psem.at[ph, k], qsem.at[ph, k], partner).start()
-        for k in range(8):
-            remote(pair_out.at[k, :, u], pair_in.at[k], psem.at[ph, k], qsem.at[ph, k], partner).wait()
-            for m in range(8):
-                total = pair_out[k, m, t].astype(F32) + pair_in[k, m].astype(F32)
-                s[k * u + m * t, m * u + k * t] = total.astype(BF)
-        for i in FAR_FIRST:
-            remote(s.at[lax.rem(a + i, 8)], ra.at[a], ssem.at[ph, i], rsem.at[ph, i], ring_a(i)).start()
-        total = s[a].astype(F32)
-        for i in NEAR_FIRST:
-            remote(s.at[lax.rem(a + i, 8)], ra.at[a], ssem.at[ph, i], rsem.at[ph, i], ring_a(i)).wait()
-            total = total + ra[lax.rem(a + 8 - i, 8)].astype(F32)
-        tb[...] = total.astype(BF)
-        for i in FAR_FIRST:
-            remote(tb.at[lax.rem(b + i, 8)], rb.at[b], ssem.at[ph + 1, i], rsem.at[ph + 1, i], ring_b(i)).start()
-        total = tb[b].astype(F32)
-        for i in NEAR_FIRST:
-            remote(tb.at[lax.rem(b + i, 8)], rb.at[b], ssem.at[ph + 1, i], rsem.at[ph + 1, i], ring_b(i)).wait()
-            total = total + rb[lax.rem(b + 8 - i, 8)].astype(F32)
-        return total
+        sp, rp, sa, ra_, sb, rb_ = (gsem.at[g, n] for n in range(6))
+        order = (*FAR_FIRST, 0)
+
+        def pair(k):
+            remote(pair_out.at[u, k], pair_in.at[k], sp.at[k], rp.at[k], partner).wait()
+            sums[k] = (pair_out[t, k].astype(F32) + pair_in[k].astype(F32)).astype(BF)
+            for i in FAR_FIRST:
+                remote(sums.at[k, lax.rem(a + i, 8)], ra.at[k, i], sa.at[k], ra_.at[k], ring_a(i)).start()
+
+        for n, k in enumerate(order):
+            rows = wd[:, lax.rem(y + k, 8), 0].reshape(128, HID)
+            pair_out[0, k] = dot(rows, hidden, 1, 0).astype(BF).reshape(8, 16, 128)
+            rows = wd[lax.rem(z + k, 8), :, 1].reshape(128, HID)
+            pair_out[1, k] = dot(rows, hidden, 1, 0).astype(BF).reshape(8, 16, 128)
+            remote(pair_out.at[u, k], pair_in.at[k], sp.at[k], rp.at[k], partner).start()
+            if n >= 4:
+                pair(order[n - 4])
+        for k in order[4:]:
+            pair(k)
+        last = None
+        for k in order:
+            seven = ra.at[k, pl.ds(1, 7)]
+            remote(seven, seven, sa.at[k], ra_.at[k], ring_a(1)).wait()
+            total = sums[k, a].astype(F32)
+            for i in range(1, 8):
+                total = total + ra[k, i].astype(F32)
+            if k == 0:
+                last = total
+            else:
+                tb[k] = total.astype(BF)
+                remote(tb.at[k], rb.at[k], sb.at[k], rb_.at[k], ring_b(k)).start()
+        if g == 1:
+            relay(2)
+        for k in NEAR_FIRST:
+            remote(tb.at[k], rb.at[k], sb.at[k], rb_.at[k], ring_b(k)).wait()
+            last = last + rb[k].astype(F32)
+        return last
 
     loads[0].wait()
     pl.semaphore_wait(barrier, 15)
@@ -201,8 +254,10 @@
             win_bc[:, :, k, :] = window[:, :, k // 2, lanes]
 
     gather_features(0, xt1, None, work1)
+    loads[19].wait()
+    relay(1)
     tokens_t = xt1[z, y, t].astype(F32)
-    sum1 = mlp(2, xt1, wt1, wd1, pair_out1, pair_in1, s1, ra1, t1, rb1)
+    sum1 = mlp(1, xt1, wt1, wd1, pair_out1, pair_in1, s1, ra1, t1, rb1)
     first = (tokens_t + 0.5 * sum1).astype(BF)
 
     af[t] = first
@@ -228,18 +283,20 @@
     put(0, dot(left, proj_z[...], 1, 0))
     put(1024, dot(left, proj_x[...], 1, 0))
     put(2048, dot(left, proj_bc[...], 1, 0))
-    last = jnp.concatenate([dot(left, proj_dt[...], 1, 1), squares, jnp.zeros((128, 111), F32)], axis=1)
+    last = [dot(left, proj_dt[...], 1, 1), squares, jnp.zeros((128, 15), F32), rows32, jnp.zeros((128, 64), F32)]
+    last = jnp.concatenate(last, axis=1)
     put(2560, last)
     for i in FAR_FIRST:
         remote(proj_s.at[lax.rem(a + i, 8)], proj_r.at[a], ssem.at[4, i], rsem.at[4, i], ring_a(i)).start()
     loads[18].wait()
     for i in NEAR_FIRST:
         remote(proj_s.at[lax.rem(a + i, 8)], proj_r.at[a], ssem.at[4, i], rsem.at[4, i], ring_a(i)).wait()
+    proj_r[a] = proj_s[a]
     for k in range(21):
         lanes = pl.ds(128 * k, 128)
-        total = proj_s[a, :, lanes].astype(F32)
-        for i in NEAR_FIRST:
-            total = total + proj_r[lax.rem(a + 8 - i, 8), :, lanes].astype(F32)
+        total = proj_r[0, :, lanes].astype(F32)
+        for i in range(1, 8):
+            total = total + proj_r[i, :, lanes].astype(F32)
         quad[:, k, :] = total
     quad[:, 21:24, :] = jnp.zeros((16, 3, 128), F32)
     quad_b[:, :24, :] = quad[...].astype(BF)
@@ -248,6 +305,15 @@
         remote(
             quad_b.at[pl.ds(2 * lax.rem(b + i, 8), 2)], quad_r.at[b], ssem.at[5, i], rsem.at[5, i], ring_b(i)
         ).start()
+    relay(3)
+
+    def first_columns():
+        tail = [proj_r[i, :, pl.ds(2560, 128)][:, 32:64] for i in range(8)]
+        af_q[0] = jnp.concatenate(tail[:4], axis=1)
+        af_q[1] = jnp.concatenate(tail[4:], axis=1)
+        remote(af_q.at[0], af_q.at[0], psem.at[6, 0], qsem.at[6, 0], partner).start()
+
+    pl.when(t == 1)(first_columns)
     full = quad[pl.ds(2 * b, 2)]
     for i in NEAR_FIRST:
         remote(
@@ -255,6 +321,7 @@
         ).wait()
         full = full + quad_r[lax.rem(b + 8 - i, 8)].astype(F32)[:, :24, :]
 
+    relay(4)
     head_of_row = iota((8, 16), 0)
     head = iota((8, 16), 1)
     lane = iota((8, 128), 1)
@@ -309,10 +376,10 @@
         blocks.append(gated * scale * group_gain[...])
     mixed = jnp.concatenate(blocks, axis=0).astype(BF)
 
-    mix_a[b] = mixed
+    mix_a[z] = mixed
     for i in FAR_FIRST:
-        remote(mix_a.at[b], mix_a.at[b], ssem.at[6, i], rsem.at[6, i], ring_b(i)).start()
-    for load in loads[19:]:
+        remote(mix_a.at[z], mix_a.at[z], ssem.at[6, i], rsem.at[6, i], ring_z(i)).start()
+    for load in loads[20:]:
         load.wait()
     prepare(gate2, up2, down2, gain2, wt2, wd2)
     packed = jnp.concatenate([kept[0][3], kept[1][3], kept[0][4], kept[1][4]], axis=0).T
@@ -336,31 +403,47 @@
     ]
     for store in stores:
         store.start()
+    pl.when(t == 1)(lambda: remote(af_q.at[0], af_q.at[0], psem.at[6, 0], qsem.at[6, 0], partner).wait_send())
+    pl.when(t == 0)(lambda: remote(af_q.at[0], af_q.at[0], psem.at[6, 0], qsem.at[6, 0], partner).wait_recv())
+    relay_end()
     for i in NEAR_FIRST:
-        remote(mix_a.at[b], mix_a.at[b], ssem.at[6, i], rsem.at[6, i], ring_b(i)).wait()
+        remote(mix_a.at[z], mix_a.at[z], ssem.at[6, i], rsem.at[6, i], ring_z(i)).wait()
     mix_f[...] = mix_a[...].reshape(128, 128).astype(F32)
-    for k in range(8):
-        mix_x[a, :, pl.ds(128 * k, 128)] = mix_f[pl.ds(k, 16, stride=8), :].astype(BF)
-    for i in FAR_FIRST:
-        remote(mix_x.at[a], mix_x.at[a], ssem.at[7, i], rsem.at[7, i], ring_a(i)).start()
-    for i in NEAR_FIRST:
-        remote(mix_x.at[a], mix_x.at[a], ssem.at[7, i], rsem.at[7, i], ring_a(i)).wait()
-    partial = dot(out_w[...], mix_x[...].reshape(128, 1024), 1, 1).astype(BF)
-    halves = dot(partial, perm, 1, 0)
-    out_s[...] = halves.astype(BF).reshape(2, 16, 128)
+    mixed_rows = jnp.concatenate([mix_f[pl.ds(k, 16, stride=8), :].astype(BF) for k in range(8)], axis=1)
+    partial = dot(mixed_rows, out_w[...].reshape(256, 1024), 1, 1).astype(BF)
+    out_s[0] = partial[:, :128]
+    out_s[1] = partial[:, 128:]
     swap = remote(out_s.at[u], out_r, psem.at[5, 0], qsem.at[5, 0], partner)
     swap.start()
     swap.wait()
     mixed_sum = out_s[t].astype(F32) + out_r[...].astype(F32)
-    after = (first.astype(F32) + mixed_sum).astype(BF)
-
-    gather_features(8, xt2, after)
-    sum2 = mlp(10, xt2, wt2, wd2, pair_out2, pair_in2, s2, ra2, t2, rb2)
-    result_v[...] = (after.astype(F32) + 0.5 * sum2).astype(BF)
+    after = (af_q[t].astype(F32) + mixed_sum).astype(BF)
+
+    gather_features(2, xt2, after)
+    own_lane = lax.rem(y, 4) * 32 + t * 16
+    chosen = (iota((16, 128), 1) == iota((16, 128), 0) + own_lane).astype(BF)
+    after_t = dot(chosen, xt2[z, :, y // 4].reshape(128, 128), 1, 1)
+    sum2 = mlp(3, xt2, wt2, wd2, pair_out2, pair_in2, s2, ra2, t2, rb2)
+    result_v[...] = dot((after_t + 0.5 * sum2).astype(BF), (swapped == col).astype(BF), 1, 0).astype(BF)
     stores.append(pltpu.make_async_copy(result_v, result_o, local_sem.at[3]))
     stores[3].start()
     for store in stores:
         store.wait()
+
+
+def finish(result_h, state_h, win_x_h, win_bc_h, result_o, state_o, win_x_o, win_bc_o, result, state, win_x, win_bc, sem):
+    moves = [(state_h.at[k // 4, pl.ds(2 * (k % 4), 2)], state.at[k // 4, pl.ds(2 * (k % 4), 2)],
+              state_o.at[k // 4, pl.ds(2 * (k % 4), 2)]) for k in range(8)]
+    moves += [(result_h, result, result_o), (win_x_h, win_x, win_x_o), (win_bc_h, win_bc, win_bc_o)]
+    ins = [pltpu.make_async_copy(src, mid, sem.at[0, n]) for n, (src, mid, _) in enumerate(moves)]
+    outs = [pltpu.make_async_copy(mid, dst, sem.at[1, n]) for n, (_, mid, dst) in enumerate(moves)]
+    for copy in ins:
+        copy.start()
+    for n in range(len(moves)):
+        ins[n].wait()
+        outs[n].start()
+    for copy in outs:
+        copy.wait()
 
 
 def per_device(
@@ -380,16 +463,17 @@
     dma = pltpu.SemaphoreType.DMA
     tile = (16, 128)
     scratch = [pltpu.VMEM(v.shape, v.dtype) for v in inputs[1:]]
+    scratch[18] = pltpu.VMEM((8, 32, 1024), BF)
     scratch += [
         pltpu.VMEM((32, 512), BF), pltpu.VMEM((4, 8, 128), F32), pltpu.VMEM((4, 4, 128), F32),
         pltpu.VMEM((2, 3, 8, 128), F32), pltpu.VMEM((2, 3, 4, 128), F32),
         pltpu.VMEM((2, 8, 128, 128), F32), pltpu.VMEM((3, 2, 1024), BF), pltpu.VMEM((2, 3, 2, 256), BF),
         pltpu.VMEM((16, 128), BF),
-        pltpu.VMEM((2, HID, 2048), BF), pltpu.VMEM((2048, HID), BF),
-        pltpu.VMEM((2, HID, 2048), BF), pltpu.VMEM((2048, HID), BF),
+        pltpu.VMEM((2, HID, 2048), BF), pltpu.VMEM((8, 8, 2, 16, HID), BF),
+        pltpu.VMEM((2, HID, 2048), BF), pltpu.VMEM((8, 8, 2, 16, HID), BF),
         pltpu.VMEM((8, 8, 2, *tile), BF), pltpu.VMEM((8, 8, 2, *tile), BF),
-        pltpu.VMEM((8, 8, 2, *tile), BF), pltpu.VMEM((8, 8, *tile), BF),
-        pltpu.VMEM((8, 8, 2, *tile), BF), pltpu.VMEM((8, 8, *tile), BF),
+        pltpu.VMEM((2, 8, 8, *tile), BF), pltpu.VMEM((8, 8, *tile), BF),
+        pltpu.VMEM((2, 8, 8, *tile), BF), pltpu.VMEM((8, 8, *tile), BF),
         pltpu.VMEM((8, 8, *tile), BF), pltpu.VMEM((8, 8, *tile), BF),
         pltpu.VMEM((8, 8, *tile), BF), pltpu.VMEM((8, 8, *tile), BF),
         pltpu.VMEM((8, *tile), BF), pltpu.VMEM((8, *tile), BF),
@@ -397,11 +481,11 @@
         pltpu.VMEM((2, *tile), BF),
         pltpu.VMEM((8, 16, WIDE), BF), pltpu.VMEM((8, 16, WIDE), BF),
         pltpu.VMEM((16, 24, 128), F32), pltpu.VMEM((16, 32, 128), BF), pltpu.VMEM((8, 2, 32, 128), BF),
-        pltpu.VMEM((8, *tile), BF), pltpu.VMEM((128, 128), F32), pltpu.VMEM((8, 16, 1024), BF),
+        pltpu.VMEM((8, *tile), BF), pltpu.VMEM((128, 128), F32), pltpu.VMEM((2, *tile), BF),
         pltpu.VMEM((2, *tile), BF), pltpu.VMEM(tile, BF),
-        dma((24,)), dma((4,)), dma((12, 8)), dma((12, 8)), dma((12, 8)), dma((12, 8)),
+        dma((24,)), dma((4,)), dma((8, 8)), dma((8, 8)), dma((8, 8)), dma((8, 8)), dma((4, 6, 8)), dma((2, 5)), dma((2, 5)),
     ]
-    result, new_state, new_x, new_bc = pl.pallas_call(
+    results = pl.pallas_call(
         kernel,
         out_shape=outs,
         in_specs=[hbm] * len(inputs),
@@ -411,6 +495,14 @@
             collective_id=1, has_side_effects=True, vmem_limit_bytes=67043328
         ),
     )(*inputs)
+    result, new_state, new_x, new_bc = pl.pallas_call(
+        finish,
+        out_shape=outs,
+        in_specs=[hbm] * len(outs),
+        out_specs=[hbm] * len(outs),
+        scratch_shapes=[pltpu.VMEM(v.shape, v.dtype) for v in outs] + [dma((2, 11))],
+        compiler_params=pltpu.CompilerParams(vmem_limit_bytes=67043328),
+    )(*results)
     return (result.T, new_state.reshape(2, 16, 64, 128), new_x.transpose(1, 0, 2), new_bc)
 
 

time: 102 us -> 88.7 us (0.87)
  Pallas kernels: 96.4 us -> 87.5 us
  local copies, waits for them, and re-layouts: 4.87 us -> 0 us
    pallas_call x1, Pallas kernels: 96.4 us -> 85.4 us  [per_device(): pl.pallas_call(kernel, out_shape=outs, in_specs=[hbm] * len(inputs), out_...]
    unnamed x10 -> x0, local copies, waits for them, and re-layouts: 4.87 us -> none
    pallas_call x0 -> x1, Pallas kernels: none -> 2.15 us  [per_device(): pl.pallas_call(finish, out_shape=outs, in_specs=[hbm] * len(outs), out_sp...]
where the time goes in v2:
time: 88.7 us; the launch traced here: 88.2 us
  Pallas kernels  87.5 us (99%)
    pallas_call x1, Pallas kernels, per_device(): pl.pallas_call(kernel, out_shape=outs, in_specs=[hbm] * len(inputs), out_...  85.4 us
    pallas_call x1, Pallas kernels, per_device(): pl.pallas_call(finish, out_shape=outs, in_specs=[hbm] * len(outs), out_sp...  2.15 us

profile of v2, /device:TPU:1, one launch (start us, length us, event | category | flops | bytes accessed | tf_op | source)
XLA Modules:
  0.0 88.2 jit_solution(11042785289797724989)
XLA Ops:
  0.6 85.4 %shard_map.255 = (bf16[16,128]{1,0:T(8,128)(2,1)}, f32[2,8,128,128]{3,2,1,0:T(8,128)}, bf16[3,2,1024]{2,1,0:T(2,128)(2,1)}, bf16[2,3,2,256]{3,2,1,0:T(2,128)(2,1)}) custom-call(bf16[16,128]{1,0:T(8,128)(2,1)} %bitcast.29, bf16[44,2048]{1,0:T(8,128)(2,1)} %bitcast.20, bf16[44,2048]{1,0:T(8,128)(2,1)} %bitcast.21, bf16[44,2048]{1,0:T(8,128)(2,1)} %down1_h.1, ...), custom_call_target="tpu_custom_call" | custom-call | tf_op jit(solution)/shard_map/pallas_call | solution.py:488
  86.0 2.1 %shard_map.256 = (bf16[16,128]{1,0:T(8,128)(2,1)}, f32[2,8,128,128]{3,2,1,0:T(8,128)}, bf16[3,2,1024]{2,1,0:T(2,128)(2,1)}, bf16[2,3,2,256]{3,2,1,0:T(2,128)(2,1)}) custom-call(bf16[16,128]{1,0:T(8,128)(2,1)} %get-tuple-element.12.result_h, f32[2,8,128,128]{3,2,1,0:T(8,128)} %get-tuple-element.13.state_h, bf16[3,2,1024]{2,1,0:T(2,128)(2,1)} %get-tuple-element.14.win_x_h, ...), custom_call_target="tpu_custom_call" | custom-call | tf_op jit(solution)/shard_map/pallas_call | solution.py:498
